TPU v7x, 128 devices: a whole 4x4x4 slice. The times are simulated.
128 devices in a mesh: sp: 64 (over z, y, x), tp: 2 (over core).
Axes of the slice: x: 4, y: 4, z: 4, core: 2. Of those that a mesh axis runs over, the one named last changes fastest.
Arguments:
- pool_input: bfloat16 [16384, 1024], P('sp', 'tp'), may hold values from -6 to 6
- residual: bfloat16 [16384, 2048], P(('sp', 'tp')), may hold values from -6 to 6
- pool_weight: bfloat16 [4, 256, 256], replicated, may hold values from -0.375 to 0.375
- pool_gain: float32 [1024], replicated, may hold values from 0.1 to 1.9
- out_weight: bfloat16 [1024, 2048], replicated, may hold values from -0.1875 to 0.1875
- norm_gain: float32 [2048], replicated, may hold values from 0.1 to 1.9
- routes: int32 [16384, 4], P(('sp', 'tp')), may hold values from 0 to 63, all different within a row; in each aligned block of 128 rows (0 to 127, 128 to 255, ...) at most 16 rows name the same one
- route_scores: float32 [16384, 4], P(('sp', 'tp')), may hold values from -1 to 1
- gate_weight: bfloat16 [64, 2048, 2048], P('sp', None, 'tp'), may hold values from -0.375 to 0.375
- up_weight: bfloat16 [64, 2048, 2048], P('sp', None, 'tp'), may hold values from -0.375 to 0.375
- down_weight: bfloat16 [64, 2048, 2048], P('sp', 'tp'), may hold values from -0.0234375 to 0.0234375
Outputs:
- layer_out: bfloat16 [16384, 2048], P(('sp', 'tp'))
Inputs may be any that keep to these rules, and one draw needn't show every extreme that they name: `routes`: each row names 4 different experts; among the rows of one device no expert is named more than 16 times, a bound that some block reaches.
All inputs are finite; a program needn't handle non-finite values.
Results may differ from a plain program's by a relative error of at most 0.012.
Values may be sent and summed in bfloat16 or wider, within the bound.
No kernel may reach another device: no remote copies, remote signals or barrier semaphores. Data moves between devices by JAX's collectives and lax.ppermute only.
A program may use at most 128 MiB of HBM per device.

v0:
```python
import jax
import jax.numpy as jnp
from jax import lax
from jax.sharding import PartitionSpec as P


def from_behind(block, axis, distance):
    devices = range(lax.axis_size(axis))
    route = [(i - distance, i) for i in devices if i - distance in devices]
    return lax.ppermute(block, axis, route)


def in_blocks(x, dim, devices):
    before, after = (x.shape[:dim], x.shape[dim + 1 :])
    return jnp.moveaxis(x.reshape(*before, devices, -1, *after), dim, 0)


def sent_and_summed(x, axis, dim):
    devices = lax.axis_size(axis)
    parts = lax.all_to_all(in_blocks(x, dim, devices), axis, 0, 0, tiled=True)
    return jnp.sum(parts.astype(jnp.float32), axis=0)


def expert_half(rows, gate_local, up_local, down_local):
    gate_pre = jnp.dot(rows, gate_local, preferred_element_type=jnp.float32)
    up_pre = jnp.dot(rows, up_local, preferred_element_type=jnp.float32)
    clipped_gate = jnp.minimum(gate_pre, 7.0)
    clipped_up = jnp.clip(up_pre, -7.0, 7.0)
    activated = ((clipped_up + 1.0) * (clipped_gate * jax.nn.sigmoid(1.702 * clipped_gate))).astype(
        jnp.bfloat16
    )
    return jnp.dot(activated, down_local, preferred_element_type=jnp.float32).astype(jnp.bfloat16)


def shards(
    pool_input,
    residual,
    pool_weight,
    pool_gain,
    out_weight,
    norm_gain,
    routes,
    route_scores,
    gate_weight,
    up_weight,
    down_weight,
):
    tokens_here, width_here = pool_input.shape
    cores = lax.axis_size("tp")
    groups_here = pool_weight.shape[0] // cores
    group_dim = pool_weight.shape[1]
    core_index = lax.axis_index("tp")
    first_group = core_index * groups_here
    previous = from_behind(pool_input[tokens_here - 16 :], "sp", 1)
    extended = jnp.concatenate([previous, pool_input], axis=0).astype(jnp.float32)
    channel_group = first_group + jnp.arange(width_here) // group_dim
    windows = jnp.left_shift(jnp.int32(2), channel_group).astype(jnp.float32)
    totals = jnp.zeros((tokens_here, width_here), jnp.float32)
    for offset in range(16):
        keeper = (windows > offset).astype(jnp.float32)
        totals = totals + extended[16 - offset : 16 - offset + tokens_here] * keeper[None, :]
    positions = (lax.axis_index("sp") * tokens_here + jnp.arange(tokens_here)).astype(jnp.float32)
    counts = jnp.minimum(positions[:, None] + 1.0, windows[None, :])
    pooled = (totals / counts - pool_input.astype(jnp.float32)).astype(jnp.bfloat16)
    local_weight = lax.dynamic_slice_in_dim(pool_weight, first_group, groups_here, 0)
    local_gain = lax.dynamic_slice_in_dim(pool_gain, first_group * group_dim, width_here, 0)
    grouped = jnp.einsum(
        "tgc,gce->tge",
        pooled.reshape(tokens_here, groups_here, group_dim),
        local_weight,
        preferred_element_type=jnp.float32,
    )
    mixer_out = (grouped.reshape(tokens_here, width_here) * local_gain[None, :]).astype(
        jnp.bfloat16
    )
    token_rows = lax.all_to_all(mixer_out, "tp", split_axis=0, concat_axis=1, tiled=True)
    projected = jnp.dot(token_rows, out_weight, preferred_element_type=jnp.float32)
    middle = (residual.astype(jnp.float32) + projected).astype(jnp.bfloat16)
    middle_wide = middle.astype(jnp.float32)
    normed = (
        middle_wide
        * lax.rsqrt(jnp.mean(middle_wide * middle_wide, axis=1, keepdims=True) + 1e-05)
        * norm_gain[None, :]
    ).astype(jnp.bfloat16)
    weights = jax.nn.softmax(route_scores, axis=-1)
    row_count, top_count = routes.shape
    model_width = normed.shape[1]
    experts_total = gate_weight.shape[0] * lax.axis_size("sp")
    capacity = row_count * top_count * cores // experts_total
    slots_total = experts_total * capacity
    flat_expert = routes.reshape(-1)
    onehot = (flat_expert[:, None] == jnp.arange(experts_total)[None, :]).astype(jnp.int32)
    ranks = jnp.sum((jnp.cumsum(onehot, axis=0) - 1) * onehot, axis=1)
    slot_ids = flat_expert * capacity + ranks
    picker = jnp.any(
        (jnp.arange(slots_total)[:, None] == slot_ids[None, :]).reshape(
            slots_total, row_count, top_count
        ),
        axis=2,
    ).astype(jnp.bfloat16)
    outgoing = (
        jnp.dot(picker, normed, preferred_element_type=jnp.float32)
        .astype(jnp.bfloat16)
        .reshape(experts_total, capacity, model_width)
    )
    gate_local = gate_weight[0]
    up_local = up_weight[0]
    down_local = down_weight[0]
    paired = lax.all_gather(
        lax.all_to_all(outgoing, "sp", split_axis=0, concat_axis=0, tiled=True),
        "tp",
        axis=0,
        tiled=True,
    )
    partial_value = expert_half(
        paired.reshape(-1, model_width), gate_local, up_local, down_local
    ).reshape(paired.shape)
    summed = sent_and_summed(partial_value, "tp", 0).astype(jnp.bfloat16)
    expert_out = lax.all_to_all(summed, "sp", split_axis=0, concat_axis=0, tiled=True)
    expert_flat = expert_out.reshape(slots_total, model_width)
    route_rows = (
        expert_flat[slot_ids].astype(jnp.float32).reshape(row_count, top_count, model_width)
    )
    mixture = jnp.sum(route_rows * weights[:, :, None], axis=1)
    return (middle_wide + mixture).astype(jnp.bfloat16)


def solution(mesh):
    return jax.shard_map(
        shards,
        mesh=mesh,
        in_specs=(
            P("sp", "tp"),
            P(("sp", "tp"), None),
            P(),
            P(),
            P(),
            P(),
            P(("sp", "tp"), None),
            P(("sp", "tp"), None),
            P("sp", None, "tp"),
            P("sp", None, "tp"),
            P("sp", "tp", None),
        ),
        out_specs=P(("sp", "tp"), None),
        check_vma=False,
    )
```

profile of v0, /device:TPU:0, one launch (start us, length us, event | category | flops | bytes accessed | tf_op | source)
XLA Modules:
  0.0 270.4 jit_solution(11678458812910446133)
XLA Ops:
  6.5 0.8 slice.57
  7.3 3.5 %collective-permute-start = (bf16[16,512]{1,0:T(8,128)(2,1)S(1)}, bf16[16,512]{1,0:T(8,128)(2,1)S(1)}, u32[]{:S(2)}, u32[]{:S(2)}) collective-permute-start(bf16[16,512]{1,0:T(8,128)(2,1)S(1)} %slice.57), channel_id=1, source_target_pairs={{0,2},{2,4},{4,6},{6,8},{8,10},{10,12},{12,14},{14,16},{16,18},{18... | collective-permute-start | bytes 49160 | tf_op jit(solution)/shard_map/ppermute | solution.py:10
  11.0 0.8 copy.35
  12.0 1.2 reduce-window.6
  13.8 0.4 fusion.11
  14.2 0.8 dynamic_slice.7
  15.0 1.0 maximum_convert_fusion
  16.0 2.0 fusion.32
  18.0 0.3 convolution_bitcast_fusion
  18.7 3.9 %all_to_all.31 = bf16[2,128,512]{1,2,0:T(8,128)(2,1)S(1)} all-to-all(bf16[2,128,512]{1,2,0:T(8,128)(2,1)S(1)} %fusion.29), channel_id=1, replica_groups=mesh['sp'=64,'tp'=2] {'tp'}, dimensions={0} | all-to-all | bytes 524288 | tf_op jit(solution)/shard_map/all_to_all | solution.py:76
  22.6 3.0 %multiply_reduce_fusion.1 = (f32[128]{0:T(128)S(1)}, f32[128,2048]{1,0:T(8,128)S(1)}) fusion(bf16[128,1024]{0,1:T(8,128)(2,1)S(1)} %bitcast.49, bf16[1024,2048]{1,0:T(8,128)(2,1)} %param.15, bf16[128,2048]{1,0:T(8,128)(2,1)S(1)} %copy-done.2), kind=kOutput, calls=%fused_computation.21 | convolution fusion | flops 538443648 | bytes 6029824 | tf_op jit(solution)/shard_map/dot_general | solution.py:77
  25.7 1.3 convolution_convert_fusion.1
  27.0 63.9 %all_to_all.32 = bf16[64,16,2048]{2,1,0:T(8,128)(2,1)} all-to-all(bf16[64,16,2048]{2,1,0:T(8,128)(2,1)S(1)} %bitcast.47), channel_id=1, replica_groups=mesh['sp'=64,'tp'=2] {'sp'}, dimensions={0} | all-to-all | bytes 8388608 | tf_op jit(solution)/shard_map/all_to_all | solution.py:110
  90.9 19.3 %all-gather.2.cloned.1.call-done = bf16[128,16,2048]{2,1,0:T(8,128)(2,1)} async-done(((bf16[64,16,2048]{2,1,0:T(8,128)(2,1)}), bf16[128,16,2048]{2,1,0:T(8,128)(2,1)}) %all-gather.2.cloned.1.call-update) | async-done | bytes 8388624 | tf_op jit(solution)/shard_map/all_gather | solution.py:109
  110.3 14.4 %fusion.1 = f32[2048,1024]{1,0:T(8,128)} fusion(bf16[2048,2048]{1,0:T(8,128)(2,1)} %bitcast.53, bf16[1,2048,1024]{2,1,0:T(8,128)(2,1)} %param.19), kind=kOutput, calls=%fused_computation.4 | convolution fusion | flops 8589934592 | bytes 20971520 | tf_op jit(solution)/shard_map/dot_general | solution.py:25
  124.7 26.9 %convolution_convert_fusion = bf16[2048,2048]{1,0:T(8,128)(2,1)} fusion(f32[2048,1024]{1,0:T(8,128)} %fusion.1, bf16[2048,2048]{1,0:T(8,128)(2,1)} %bitcast.54, bf16[1,1024,2048]{2,1,0:T(8,128)(2,1)} %param.21, bf16[1,2048,1024]{2,1,0:T(8,128)(2,1)} %param.20), kind=kOutput, calls=%fused_computation.2 | convolution fusion | flops 17205035008 | bytes 33554432 | tf_op jit(solution)/shard_map/dot_general | solution.py:32
  151.6 18.5 %all_to_all.33 = bf16[2,64,16,2048]{3,2,1,0:T(8,128)(2,1)} all-to-all(bf16[2,64,16,2048]{3,2,1,0:T(8,128)(2,1)} %bitcast.48), channel_id=1, replica_groups=mesh['sp'=64,'tp'=2] {'tp'}, dimensions={0} | all-to-all | bytes 16777216 | tf_op jit(solution)/shard_map/all_to_all | solution.py:20
  170.1 8.9 %reduce_sum.55 = bf16[64,16,2048]{2,1,0:T(8,128)(2,1)} reduce(bf16[2,64,16,2048]{3,2,1,0:T(8,128)(2,1)} %all_to_all.33, bf16[]{:T(256)} %constant.130.clone.1), dimensions={0}, to_apply=%region_5.6 | reduce | flops 2097152 | bytes 12582914 | tf_op jit(solution)/shard_map/reduce_sum | solution.py:21
  179.0 10.8 %all-to-all-start.3 = ((bf16[64,16,2048]{2,1,0:T(8,128)(2,1)}), bf16[64,16,2048]{2,1,0:T(8,128)(2,1)}, u32[]{:S(2)}, u32[]{:S(2)}) async-start(bf16[64,16,2048]{2,1,0:T(8,128)(2,1)} %reduce_sum.55), calls=%async_computation.3 | async-start | bytes 8388608 | tf_op jit(solution)/shard_map/all_to_all | solution.py:119
  190.1 54.2 %all-to-all-done.3 = bf16[64,16,2048]{2,1,0:T(8,128)(2,1)} async-done(((bf16[64,16,2048]{2,1,0:T(8,128)(2,1)}), bf16[64,16,2048]{2,1,0:T(8,128)(2,1)}, u32[]{:S(2)}, u32[]{:S(2)}) %all-to-all-start.3) | async-done | bytes 4194336 | tf_op jit(solution)/shard_map/all_to_all | solution.py:119
  244.4 8.0 %gather_fusion = bf16[512,2048]{1,0:T(8,128)(2,1)} fusion(bf16[1024,2048]{1,0:T(8,128)(2,1)} %bitcast.10, s32[1024]{0:T(1024)S(1)} %pad_clamp_fusion), kind=kCustom, calls=%fused_computation | custom fusion | bytes 4196352 | tf_op jit(solution)/shard_map/gather | solution.py:122
  252.4 4.8 %reshape.199 = f32[128,4,2048]{2,1,0:T(4,128)} reshape(bf16[512,2048]{1,0:T(8,128)(2,1)} %gather_fusion) | data formatting | bytes 6291456 | tf_op jit(solution)/shard_map/convert_element_type | solution.py:122
  257.2 5.4 %multiply_reduce_fusion = f32[128,2048]{1,0:T(8,128)S(1)} fusion(f32[128,4,2048]{2,1,0:T(4,128)} %reshape.199, f32[128,4]{1,0:T(8,128)S(1)} %copy.40), kind=kLoop, calls=%fused_computation.7 | loop fusion | flops 1835008 | bytes 5244928 | tf_op jit(solution)/shard_map/reduce_sum | solution.py:124
  262.6 0.9 add_convert_fusion
  (43 shorter events, 1.6 us)
Async XLA Ops:
  6.5 11.4 %copy-start = (bf16[4,256,256]{2,1,0:T(8,128)(2,1)S(1)}, bf16[4,256,256]{2,1,0:T(8,128)(2,1)}, u32[]{:S(2)}) copy-start(bf16[4,256,256]{2,1,0:T(8,128)(2,1)} %param.13) | copy-start | bytes 1572868
  6.5 103.7 %all-gather.2.cloned.1.call-start = ((), (), s32[]{:S(2)}) async-start(), calls=%async_computation.4 | async-start | bytes 12582912 | tf_op jit(solution)/shard_map/all_gather | solution.py:109
  7.3 7.6 %collective-permute-start = (bf16[16,512]{1,0:T(8,128)(2,1)S(1)}, bf16[16,512]{1,0:T(8,128)(2,1)S(1)}, u32[]{:S(2)}, u32[]{:S(2)}) collective-permute-start(bf16[16,512]{1,0:T(8,128)(2,1)S(1)} %slice.57), channel_id=1, source_target_pairs={{0,2},{2,4},{4,6},{6,8},{8,10},{10,12},{12,14},{14,16},{16,18},{18... | collective-permute-start | bytes 49160 | tf_op jit(solution)/shard_map/ppermute | solution.py:10
  16.0 6.7 %copy-start.2 = (bf16[128,2048]{1,0:T(8,128)(2,1)S(1)}, bf16[128,2048]{1,0:T(8,128)(2,1)}, u32[]{:S(2)}) copy-start(bf16[128,2048]{1,0:T(8,128)(2,1)} %param.12) | copy-start | bytes 1572868
  18.3 7.4 %copy-start.4 = (f32[2048]{0:T(1024)S(1)}, f32[2048]{0:T(1024)}, u32[]{:S(2)}) copy-start(f32[2048]{0:T(1024)} %param.16) | copy-start | bytes 24580
  179.0 10.9 %copy-start.3 = (f32[128,4]{0,1:T(4,128)S(1)}, f32[128,4]{0,1:T(4,128)}, u32[]{:S(2)}) copy-start(f32[128,4]{0,1:T(4,128)} %param.18) | copy-start | bytes 6148
  179.0 65.4 %all-to-all-start.3 = ((bf16[64,16,2048]{2,1,0:T(8,128)(2,1)}), bf16[64,16,2048]{2,1,0:T(8,128)(2,1)}, u32[]{:S(2)}, u32[]{:S(2)}) async-start(bf16[64,16,2048]{2,1,0:T(8,128)(2,1)} %reduce_sum.55), calls=%async_computation.3 | async-start | bytes 8388608 | tf_op jit(solution)/shard_map/all_to_all | solution.py:119
  252.4 11.2 %copy-start.1 = (bf16[4,256,256]{2,1,0:T(8,128)(2,1)S(1)}, bf16[4,256,256]{2,1,0:T(8,128)(2,1)}, u32[]{:S(2)}) copy-start(bf16[4,256,256]{2,1,0:T(8,128)(2,1)} %param.13) | copy-start | bytes 1572868
Sparse Core Ops, SparseCore 0:
  91.1 19.1 all-gather.1
where the time goes:
time: 271 us; the launch traced here: 270 us
  blocking collectives  86.4 us (32%)
  waiting for transfers between devices  73.6 us (27%)
  matrix products  45.9 us (17%)
  other arithmetic  20.3 us (7%)
  local copies, waits for them, and re-layouts  16.3 us (6%)
  starting transfers between devices  14.3 us (5%)
  between operations  13.6 us (5%)
    all_to_all x1, blocking collectives, shards(): lax.all_to_all(outgoing, 'sp', split_axis=0, concat_axis=0, tiled=True)  63.9 us
    all_to_all x1, waiting for transfers between devices, shards(): lax.all_to_all(summed, 'sp', split_axis=0, concat_axis=0, tiled=True)  54.2 us
    dot_general x1, matrix products, expert_half(): jnp.dot(activated, down_local, preferred_element_type=jnp.float32)  26.9 us
    all_gather x1, waiting for transfers between devices, shards(): lax.all_gather(lax.all_to_all(outgoing, 'sp', split_axis=0, concat_axis=0...  19.3 us
    all_to_all x1, blocking collectives, sent_and_summed(): parts = lax.all_to_all(in_blocks(x, dim, devices), axis, 0, 0, tiled=True)  18.5 us
    dot_general x1, matrix products, expert_half(): gate_pre = jnp.dot(rows, gate_local, preferred_element_type=jnp.float32)  14.4 us
    all_to_all x1, starting transfers between devices, shards(): lax.all_to_all(summed, 'sp', split_axis=0, concat_axis=0, tiled=True)  10.8 us
    reduce_sum x1, other arithmetic, sent_and_summed(): return jnp.sum(parts.astype(jnp.float32), axis=0)  8.89 us
  transfers between devices with their start and end apart: 3, of which 2 were waited for; matrix products, arithmetic and copies ran while one was open for 2% of the time, Pallas kernels for 0%

commit v1 on v0

--- a/solution.py
+++ b/solution.py
@@ -106,11 +106,17 @@
     gate_local = gate_weight[0]
     up_local = up_weight[0]
     down_local = down_weight[0]
-    paired = lax.all_gather(
-        lax.all_to_all(outgoing, "sp", split_axis=0, concat_axis=0, tiled=True),
-        "tp",
+    paired = jnp.concatenate(
+        lax.all_to_all(
+            jnp.stack(
+                [lax.all_to_all(outgoing, "sp", split_axis=0, concat_axis=0, tiled=True)]
+                * lax.axis_size("tp")
+            ),
+            "tp",
+            0,
+            0,
+        ),
         axis=0,
-        tiled=True,
     )
     partial_value = expert_half(
         paired.reshape(-1, model_width), gate_local, up_local, down_local

time: 271 us -> 250 us (0.923)
  waiting for transfers between devices: 73.6 us -> 54.2 us
  between operations: 13.6 us -> 0.24 us
  blocking collectives: 86.4 us -> 98.6 us
  starting transfers between devices: 14.3 us -> 9.46 us
  other arithmetic: 20.3 us -> 24.2 us
  matrix products: 45.9 us -> 42.5 us
  local copies, waits for them, and re-layouts: 16.3 us -> 19.5 us
    all_gather x1 -> x0, waiting for transfers between devices: 19.3 us -> none  [shards(): lax.all_gather(lax.all_to_all(outgoing, 'sp', split_axis=0, concat_axis=0...]
    all_to_all x0 -> x1, blocking collectives: none -> 12.3 us  [shards(): lax.all_to_all(jnp.stack([lax.all_to_all(outgoing, 'sp', split_axis=0, co...]
    all_to_all x1, starting transfers between devices: 10.8 us -> 5.97 us  [shards(): lax.all_to_all(summed, 'sp', split_axis=0, concat_axis=0, tiled=True)]
    another operation x2 -> x3, other arithmetic: 1.24 us -> 5.18 us  [the longest x1 3.94 us: shards(): jnp.stack([lax.all_to_all(outgoing, 'sp', split_axis=0, concat_axis=0, ti...]
    dot_general x1, matrix products: 14.4 us -> 11 us  [expert_half(): gate_pre = jnp.dot(rows, gate_local, preferred_element_type=jnp.float32)]
    unnamed x11 -> x15, local copies, waits for them, and re-layouts: 0.81 us -> 4.03 us
  transfers between devices with their start and end apart: 3 -> 2, of which waited for: 2 -> 1; matrix products, arithmetic and copies ran while one was open for 2% -> 2% of each run, Pallas kernels for 0% -> 0%
where the time goes in v1:
time: 250 us; the launch traced here: 249 us
  blocking collectives  98.6 us (39%)
  waiting for transfers between devices  54.2 us (22%)
  matrix products  42.5 us (17%)
  other arithmetic  24.2 us (10%)
  local copies, waits for them, and re-layouts  19.5 us (8%)
  starting transfers between devices  9.46 us (4%)
    all_to_all x1, blocking collectives, shards(): lax.all_to_all(outgoing, 'sp', split_axis=0, concat_axis=0, tiled=True)  63.8 us
    all_to_all x1, waiting for transfers between devices, shards(): lax.all_to_all(summed, 'sp', split_axis=0, concat_axis=0, tiled=True)  54.2 us
    dot_general x1, matrix products, expert_half(): jnp.dot(activated, down_local, preferred_element_type=jnp.float32)  26.9 us
    all_to_all x1, blocking collectives, sent_and_summed(): parts = lax.all_to_all(in_blocks(x, dim, devices), axis, 0, 0, tiled=True)  18.5 us
    all_to_all x1, blocking collectives, shards(): lax.all_to_all(jnp.stack([lax.all_to_all(outgoing, 'sp', split_axis=0, co...  12.3 us
    dot_general x1, matrix products, expert_half(): gate_pre = jnp.dot(rows, gate_local, preferred_element_type=jnp.float32)  11 us
    reduce_sum x1, other arithmetic, sent_and_summed(): return jnp.sum(parts.astype(jnp.float32), axis=0)  8.89 us
    gather x1, local copies, waits for them, and re-layouts, shards(): expert_flat[slot_ids].astype(jnp.float32)  8.06 us
  transfers between devices with their start and end apart: 2, of which 1 were waited for; matrix products, arithmetic and copies ran while one was open for 2% of the time, Pallas kernels for 0%

profile of v1, /device:TPU:0, one launch (start us, length us, event | category | flops | bytes accessed | tf_op | source)
XLA Modules:
  0.0 248.7 jit_solution(727511675106856724)
XLA Ops:
  0.0 0.8 slice.57
  0.8 3.5 %collective-permute-start = (bf16[16,512]{1,0:T(8,128)(2,1)S(1)}, bf16[16,512]{1,0:T(8,128)(2,1)S(1)}, u32[]{:S(2)}, u32[]{:S(2)}) collective-permute-start(bf16[16,512]{1,0:T(8,128)(2,1)S(1)} %slice.57), channel_id=1, source_target_pairs={{0,2},{2,4},{4,6},{6,8},{8,10},{10,12},{12,14},{14,16},{16,18},{18... | collective-permute-start | bytes 49160 | tf_op jit(solution)/shard_map/ppermute | solution.py:10
  4.4 0.8 copy.27
  5.5 1.2 reduce-window.6
  7.7 0.8 dynamic_slice.7
  8.5 1.0 maximum_convert_fusion
  9.5 1.9 fusion.32
  12.1 3.9 %all_to_all.36 = bf16[2,128,512]{1,2,0:T(8,128)(2,1)S(1)} all-to-all(bf16[2,128,512]{1,2,0:T(8,128)(2,1)S(1)} %fusion.29), channel_id=1, replica_groups=mesh['sp'=64,'tp'=2] {'tp'}, dimensions={0} | all-to-all | bytes 524288 | tf_op jit(solution)/shard_map/all_to_all | solution.py:76
  16.1 3.0 %multiply_reduce_fusion.1 = (f32[128]{0:T(128)S(1)}, f32[128,2048]{1,0:T(8,128)S(1)}) fusion(bf16[128,1024]{0,1:T(8,128)(2,1)S(1)} %bitcast.53, bf16[1024,2048]{1,0:T(8,128)(2,1)} %param.15, bf16[128,2048]{1,0:T(8,128)(2,1)S(1)} %copy-done.3), kind=kOutput, calls=%fused_computation.22 | convolution fusion | flops 538443648 | bytes 6029824 | tf_op jit(solution)/shard_map/dot_general | solution.py:77
  19.1 1.3 convolution_convert_fusion.1
  20.4 63.8 %all_to_all.37 = bf16[64,16,2048]{2,1,0:T(8,128)(2,1)S(1)} all-to-all(bf16[64,16,2048]{2,1,0:T(8,128)(2,1)S(1)} %bitcast.49), channel_id=1, replica_groups=mesh['sp'=64,'tp'=2] {'sp'}, dimensions={0} | all-to-all | bytes 8388608 | tf_op jit(solution)/shard_map/all_to_all | solution.py:112
  84.2 3.9 %pad_maximum_fusion = bf16[2,64,16,2048]{3,2,1,0:T(8,128)(2,1)} fusion(bf16[1,64,16,2048]{3,2,1,0:T(8,128)(2,1)S(1)} %bitcast.48), kind=kLoop, calls=%fused_computation.1 | loop fusion | flops 4194304 | bytes 12582912 | tf_op jit(solution)/shard_map/stack | solution.py:111
  88.2 12.3 %all_to_all.38 = bf16[2,64,16,2048]{3,2,1,0:T(8,128)(2,1)S(1)} all-to-all(bf16[2,64,16,2048]{3,2,1,0:T(8,128)(2,1)} %pad_maximum_fusion), channel_id=1, replica_groups=mesh['sp'=64,'tp'=2] {'tp'}, dimensions={0} | all-to-all | bytes 16777216 | tf_op jit(solution)/shard_map/all_to_all | solution.py:110
  100.5 3.2 %copy-done.2 = bf16[2,64,16,2048]{3,2,1,0:T(8,128)(2,1)} copy-done((bf16[2,64,16,2048]{3,2,1,0:T(8,128)(2,1)}, bf16[2,64,16,2048]{3,2,1,0:T(8,128)(2,1)S(1)}, u32[]{:S(2)}) %copy-start.2) | copy-done | bytes 8388632
  103.7 11.0 %fusion.1 = f32[2048,1024]{1,0:T(8,128)} fusion(bf16[2048,2048]{1,0:T(8,128)(2,1)S(1)} %bitcast.50, bf16[1,2048,1024]{2,1,0:T(8,128)(2,1)S(1)} %copy-done.6), kind=kOutput, calls=%fused_computation.5 | convolution fusion | flops 8589934592 | bytes 20971520 | tf_op jit(solution)/shard_map/dot_general | solution.py:25
  114.7 26.9 %convolution_convert_fusion = bf16[2048,2048]{1,0:T(8,128)(2,1)} fusion(f32[2048,1024]{1,0:T(8,128)} %fusion.1, bf16[2048,2048]{1,0:T(8,128)(2,1)} %bitcast.51, bf16[1,1024,2048]{2,1,0:T(8,128)(2,1)} %param.21, bf16[1,2048,1024]{2,1,0:T(8,128)(2,1)} %param.20), kind=kOutput, calls=%fused_computation.3 | convolution fusion | flops 17205035008 | bytes 33554432 | tf_op jit(solution)/shard_map/dot_general | solution.py:32
  141.6 18.5 %all_to_all.39 = bf16[2,64,16,2048]{3,2,1,0:T(8,128)(2,1)} all-to-all(bf16[2,64,16,2048]{3,2,1,0:T(8,128)(2,1)} %bitcast.52), channel_id=1, replica_groups=mesh['sp'=64,'tp'=2] {'tp'}, dimensions={0} | all-to-all | bytes 16777216 | tf_op jit(solution)/shard_map/all_to_all | solution.py:20
  160.1 8.9 %reduce_sum.55 = bf16[64,16,2048]{2,1,0:T(8,128)(2,1)} reduce(bf16[2,64,16,2048]{3,2,1,0:T(8,128)(2,1)} %all_to_all.39, bf16[]{:T(256)} %constant.130.clone.1), dimensions={0}, to_apply=%region_5.6 | reduce | flops 2097152 | bytes 12582914 | tf_op jit(solution)/shard_map/reduce_sum | solution.py:21
  169.0 6.0 %all-to-all-start.4 = ((bf16[64,16,2048]{2,1,0:T(8,128)(2,1)}), bf16[64,16,2048]{2,1,0:T(8,128)(2,1)}, u32[]{:S(2)}, u32[]{:S(2)}) async-start(bf16[64,16,2048]{2,1,0:T(8,128)(2,1)} %reduce_sum.55), calls=%async_computation.4 | async-start | bytes 8388608 | tf_op jit(solution)/shard_map/all_to_all | solution.py:125
  175.3 54.2 %all-to-all-done.4 = bf16[64,16,2048]{2,1,0:T(8,128)(2,1)} async-done(((bf16[64,16,2048]{2,1,0:T(8,128)(2,1)}), bf16[64,16,2048]{2,1,0:T(8,128)(2,1)}, u32[]{:S(2)}, u32[]{:S(2)}) %all-to-all-start.4) | async-done | bytes 4194336 | tf_op jit(solution)/shard_map/all_to_all | solution.py:125
  229.5 8.1 %gather_fusion = bf16[512,2048]{1,0:T(8,128)(2,1)} fusion(bf16[1024,2048]{1,0:T(8,128)(2,1)} %bitcast.11, s32[1024]{0:T(1024)S(1)} %pad_clamp_fusion), kind=kCustom, calls=%fused_computation | custom fusion | bytes 4196352 | tf_op jit(solution)/shard_map/gather | solution.py:128
  237.6 4.8 %reshape.195 = f32[128,4,2048]{2,1,0:T(4,128)} reshape(bf16[512,2048]{1,0:T(8,128)(2,1)} %gather_fusion) | data formatting | bytes 6291456 | tf_op jit(solution)/shard_map/convert_element_type | solution.py:128
  242.3 5.4 %multiply_reduce_fusion = f32[128,2048]{1,0:T(8,128)S(1)} fusion(f32[128,4,2048]{2,1,0:T(4,128)} %reshape.195, f32[128,4]{1,0:T(8,128)S(1)} %copy.32), kind=kLoop, calls=%fused_computation.8 | loop fusion | flops 1835008 | bytes 5244928 | tf_op jit(solution)/shard_map/reduce_sum | solution.py:130
  247.7 0.9 add_convert_fusion
  (46 shorter events, 2.3 us)
Async XLA Ops:
  0.0 11.4 %copy-start = (bf16[4,256,256]{2,1,0:T(8,128)(2,1)S(1)}, bf16[4,256,256]{2,1,0:T(8,128)(2,1)}, u32[]{:S(2)}) copy-start(bf16[4,256,256]{2,1,0:T(8,128)(2,1)} %param.13) | copy-start | bytes 1572868
  0.0 16.1 %copy-start.3 = (bf16[128,2048]{1,0:T(8,128)(2,1)S(1)}, bf16[128,2048]{1,0:T(8,128)(2,1)}, u32[]{:S(2)}) copy-start(bf16[128,2048]{1,0:T(8,128)(2,1)} %param.12) | copy-start | bytes 1572868
  0.8 7.6 %collective-permute-start = (bf16[16,512]{1,0:T(8,128)(2,1)S(1)}, bf16[16,512]{1,0:T(8,128)(2,1)S(1)}, u32[]{:S(2)}, u32[]{:S(2)}) collective-permute-start(bf16[16,512]{1,0:T(8,128)(2,1)S(1)} %slice.57), channel_id=1, source_target_pairs={{0,2},{2,4},{4,6},{6,8},{8,10},{10,12},{12,14},{14,16},{16,18},{18... | collective-permute-start | bytes 49160 | tf_op jit(solution)/shard_map/ppermute | solution.py:10
  9.5 9.6 %copy-start.5 = (f32[2048]{0:T(1024)S(1)}, f32[2048]{0:T(1024)}, u32[]{:S(2)}) copy-start(f32[2048]{0:T(1024)} %param.16) | copy-start | bytes 24580
  88.2 15.6 %copy-start.6 = (bf16[1,2048,1024]{2,1,0:T(8,128)(2,1)S(1)}, bf16[1,2048,1024]{2,1,0:T(8,128)(2,1)}, u32[]{:S(2)}) copy-start(bf16[1,2048,1024]{2,1,0:T(8,128)(2,1)} %param.19) | copy-start | bytes 12582916
  100.5 3.2 %copy-start.2 = (bf16[2,64,16,2048]{3,2,1,0:T(8,128)(2,1)}, bf16[2,64,16,2048]{3,2,1,0:T(8,128)(2,1)S(1)}, u32[]{:S(2)}) copy-start(bf16[2,64,16,2048]{3,2,1,0:T(8,128)(2,1)S(1)} %all_to_all.38) | copy-start | bytes 25165828
  160.1 15.0 %copy-start.4 = (f32[128,4]{0,1:T(4,128)S(1)}, f32[128,4]{0,1:T(4,128)}, u32[]{:S(2)}) copy-start(f32[128,4]{0,1:T(4,128)} %param.18) | copy-start | bytes 6148
  169.0 60.5 %all-to-all-start.4 = ((bf16[64,16,2048]{2,1,0:T(8,128)(2,1)}), bf16[64,16,2048]{2,1,0:T(8,128)(2,1)}, u32[]{:S(2)}, u32[]{:S(2)}) async-start(bf16[64,16,2048]{2,1,0:T(8,128)(2,1)} %reduce_sum.55), calls=%async_computation.4 | async-start | bytes 8388608 | tf_op jit(solution)/shard_map/all_to_all | solution.py:125
  229.5 19.2 %copy-start.1 = (bf16[4,256,256]{2,1,0:T(8,128)(2,1)S(1)}, bf16[4,256,256]{2,1,0:T(8,128)(2,1)}, u32[]{:S(2)}) copy-start(bf16[4,256,256]{2,1,0:T(8,128)(2,1)} %param.13) | copy-start | bytes 1572868
